TPU v7x, 32 devices: a whole 2x2x4 slice. The times are simulated.
32 devices in a mesh: fs: 8 (over z, x), tp: 4 (over y, core).
Axes of the slice: x: 2, y: 2, z: 4, core: 2. Of those that a mesh axis runs over, the one named last changes fastest.
Arguments:
- tokens: bfloat16 [2048, 2048], P('fs', 'tp'), may hold values from -6 to 6
- grad_out: bfloat16 [2048, 2048], P('fs', 'tp'), may hold values from -6 to 6
- up_weight: bfloat16 [2048, 4096], P('fs', 'tp'), may hold values from -0.125 to 0.125
- down_weight: bfloat16 [4096, 2048], P('tp', 'fs'), may hold values from -0.09375 to 0.09375
Outputs:
- input_grad: bfloat16 [2048, 2048], P('fs', 'tp')
- up_grad: float32 [2048, 4096], P('fs', 'tp')
- down_grad: float32 [4096, 2048], P('tp', 'fs')
- up_norms: float32 [2048], P('fs')
- down_norms: float32 [4096], P('tp')
All inputs are finite; a program needn't handle non-finite values.
Results may differ from a plain program's by a relative error of at most 0.015.
Values may be sent and summed in bfloat16 or wider, within the bound.
A program may use at most 64 MiB of HBM per device.

v0:
```python
import jax
import jax.numpy as jnp
from jax import lax
from jax.sharding import PartitionSpec as P


def on_device(tokens, grad_out, up_weight, down_weight):
    rows, cotan = (
        lax.all_gather(tokens, "tp", axis=1, tiled=True),
        lax.all_gather(grad_out, "tp", axis=1, tiled=True),
    )
    up_local = lax.all_gather(up_weight, "fs", axis=0, tiled=True)
    dact = lax.dot_general(
        cotan,
        lax.all_gather(down_weight, "fs", axis=1, tiled=True),
        (((1,), (1,)), ((), ())),
        preferred_element_type=jnp.float32,
    )
    pre = jnp.dot(rows, up_local, preferred_element_type=jnp.float32)
    relued = jnp.maximum(pre, 0.0)
    act = (relued * relued).astype(jnp.bfloat16)
    dpre = (dact * 2.0 * relued).astype(jnp.bfloat16)
    partial_sum = lax.dot_general(
        dpre, up_local, (((1,), (1,)), ((), ())), preferred_element_type=jnp.float32
    )
    rounded = lax.optimization_barrier(partial_sum.astype(jnp.bfloat16))
    input_grad = lax.psum_scatter(
        rounded.astype(jnp.float32).astype(jnp.bfloat16), "tp", scatter_dimension=1, tiled=True
    )
    cols = rows
    up_shard = lax.psum_scatter(
        lax.dot_general(
            cols, dpre, (((0,), (0,)), ((), ())), preferred_element_type=jnp.float32
        ).astype(jnp.bfloat16),
        "fs",
        scatter_dimension=0,
        tiled=True,
    ).astype(jnp.float32)
    cols = cotan
    down_flip = lax.psum_scatter(
        lax.dot_general(
            cols, act, (((0,), (0,)), ((), ())), preferred_element_type=jnp.float32
        ).astype(jnp.bfloat16),
        "fs",
        scatter_dimension=0,
        tiled=True,
    ).astype(jnp.float32)
    down_grad = down_flip.T
    up_norms = lax.psum(jnp.sum(up_shard * up_shard, axis=1), "tp")
    down_norms = lax.psum(jnp.sum(down_grad * down_grad, axis=1), "fs")
    return (input_grad, up_shard, down_grad, up_norms, down_norms)


def solution(mesh):
    return jax.shard_map(
        on_device,
        mesh=mesh,
        in_specs=(P("fs", "tp"), P("fs", "tp"), P("fs", "tp"), P("tp", "fs")),
        out_specs=(P("fs", "tp"), P("fs", "tp"), P("tp", "fs"), P("fs"), P("tp")),
        check_vma=False,
    )
```

profile of v0, /device:TPU:0, one launch (start us, length us, event | category | flops | bytes accessed | tf_op | source)
XLA Modules:
  0.0 419.1 jit_solution(4892946634751360285)
XLA Ops:
  7.2 0.0 all-gather.9.cloned.1.call-start
  7.2 0.7 all-gather.9.cloned.1.call-update
  7.9 0.0 all-gather.11.cloned.1.call-start
  7.9 0.7 all-gather.11.cloned.1.call-update
  8.6 0.0 all-gather.5.cloned.1.call-start
  8.7 0.7 all-gather.5.cloned.1.call-update
  9.4 0.0 all-gather.7.cloned.1.call-start
  9.4 0.5 all-gather.7.cloned.1.call-update
  10.0 0.0 reduce-scatter.6.cloned.1.call-start
  10.0 19.0 %all-gather.9.cloned.1.call-done = bf16[256,2048]{1,0:T(8,128)(2,1)} async-done(((bf16[256,512]{1,0:T(8,128)(2,1)}), bf16[256,2048]{1,0:T(8,128)(2,1)}) %all-gather.9.cloned.1.call-update) | async-done | bytes 1048592 | tf_op jit(solution)/shard_map/all_gather | solution.py:9
  29.0 74.9 %all-gather.11.cloned.1.call-done = bf16[2048,1024]{1,0:T(8,128)(2,1)} async-done(((bf16[256,1024]{1,0:T(8,128)(2,1)}), bf16[2048,1024]{1,0:T(8,128)(2,1)}) %all-gather.11.cloned.1.call-update) | async-done | bytes 4194320 | tf_op jit(solution)/shard_map/all_gather | solution.py:12
  103.9 3.8 convolution_maximum_fusion
  107.7 13.1 %all-gather.5.cloned.1.call-done = bf16[256,2048]{1,0:T(8,128)(2,1)} async-done(((bf16[256,512]{1,0:T(8,128)(2,1)}), bf16[256,2048]{1,0:T(8,128)(2,1)}) %all-gather.5.cloned.1.call-update) | async-done | bytes 1048592 | tf_op jit(solution)/shard_map/all_gather | solution.py:10
  120.8 76.6 %all-gather.7.cloned.1.call-done = bf16[1024,2048]{1,0:T(8,128)(2,1)} async-done(((bf16[1024,256]{1,0:T(8,128)(2,1)}), bf16[1024,2048]{1,0:T(8,128)(2,1)}) %all-gather.7.cloned.1.call-update) | async-done | bytes 4194320 | tf_op jit(solution)/shard_map/all_gather | solution.py:15
  197.3 3.8 fusion.1
  201.1 0.0 copy-start
  201.1 4.6 %convert_bitcast_fusion.1 = bf16[2048,1024]{0,1:T(8,128)(2,1)} fusion(bf16[256,1024]{1,0:T(8,128)(2,1)S(1)} %fusion.1, bf16[256,2048]{1,0:T(8,128)(2,1)} %all-gather.9.cloned.1.call-done), kind=kOutput, calls=%fused_computation.1 | convolution fusion | flops 1075838976 | bytes 5767168 | tf_op jit(solution)/shard_map/dot_general | solution.py:32
  205.7 0.0 reduce-scatter.6.cloned.1.call-update
  205.8 0.0 reduce-scatter.8.cloned.1.call-start
  205.8 3.3 convert_bitcast_fusion
  209.1 0.0 reduce-scatter.8.cloned.1.call-update
  209.1 0.0 reduce-scatter.4.cloned.1.call-start
  209.1 4.6 %convolution_convert_fusion = bf16[256,2048]{1,0:T(8,128)(2,1)} fusion(bf16[256,1024]{1,0:T(8,128)(2,1)S(1)} %fusion.1, bf16[2048,1024]{1,0:T(8,128)(2,1)} %all-gather.11.cloned.1.call-done), kind=kOutput, calls=%fused_computation.2 | convolution fusion | flops 1074266112 | bytes 5767168 | tf_op jit(solution)/shard_map/dot_general | solution.py:23
  213.7 0.0 reduce-scatter.4.cloned.1.call-update
  213.7 79.1 %reduce-scatter.6.cloned.1.call-done = bf16[256,1024]{0,1:T(8,128)(2,1)} async-done(((bf16[2048,1024]{0,1:T(8,128)(2,1)}), bf16[256,1024]{0,1:T(8,128)(2,1)}) %reduce-scatter.6.cloned.1.call-update) | async-done | bytes 524304 | tf_op jit(solution)/shard_map/reduce_scatter | solution.py:31
  292.8 2.2 copy.9
  295.1 1.2 multiply_reduce_fusion.1
  296.3 6.7 %psum.14 = f32[256]{0:T(256)} all-reduce(f32[256]{0:T(256)S(1)} %multiply_reduce_fusion.1), channel_id=1, replica_groups=mesh['fs'=8,'tp'=4] {'tp'}, use_global_device_ids=true, to_apply=%region_4.0 | all-reduce | flops 256 | bytes 2048 | tf_op jit(solution)/shard_map/psum | solution.py:49
  303.0 81.7 %reduce-scatter.8.cloned.1.call-done = bf16[256,1024]{0,1:T(8,128)(2,1)} async-done(((bf16[2048,1024]{0,1:T(8,128)(2,1)}), bf16[256,1024]{0,1:T(8,128)(2,1)}) %reduce-scatter.8.cloned.1.call-update) | async-done | bytes 524304 | tf_op jit(solution)/shard_map/reduce_scatter | solution.py:40
  384.7 2.1 multiply_reduce_fusion
  386.8 20.6 %psum.15 = f32[1024]{0:T(1024)} all-reduce(f32[1024]{0:T(1024)S(1)} %get-tuple-element.10), channel_id=1, replica_groups=mesh['fs'=8,'tp'=4] {'fs'}, use_global_device_ids=true, to_apply=%region_6.0 | all-reduce | flops 1024 | bytes 8192 | tf_op jit(solution)/shard_map/psum | solution.py:50
  407.4 4.8 %reduce-scatter.4.cloned.1.call-done = bf16[256,512]{1,0:T(8,128)(2,1)} async-done(((bf16[256,2048]{1,0:T(8,128)(2,1)}), bf16[256,512]{1,0:T(8,128)(2,1)}) %reduce-scatter.4.cloned.1.call-update) | async-done | bytes 262160 | tf_op jit(solution)/shard_map/reduce_scatter | solution.py:27
  (1 shorter events, 0.0 us)
Async XLA Ops:
  7.2 21.8 %all-gather.9.cloned.1.call-start = ((), (), s32[]{:S(2)}) async-start(), calls=%async_computation.5 | async-start | bytes 1310720 | tf_op jit(solution)/shard_map/all_gather | solution.py:9
  7.9 96.0 %all-gather.11.cloned.1.call-start = ((), (), s32[]{:S(2)}) async-start(), calls=%async_computation.6 | async-start | bytes 4718592 | tf_op jit(solution)/shard_map/all_gather | solution.py:12
  8.6 112.1 %all-gather.5.cloned.1.call-start = ((), (), s32[]{:S(2)}) async-start(), calls=%async_computation.3 | async-start | bytes 1310720 | tf_op jit(solution)/shard_map/all_gather | solution.py:10
  9.4 188.0 %all-gather.7.cloned.1.call-start = ((), (), s32[]{:S(2)}) async-start(), calls=%async_computation.4 | async-start | bytes 4718592 | tf_op jit(solution)/shard_map/all_gather | solution.py:15
  10.0 282.9 %reduce-scatter.6.cloned.1.call-start = ((), (), s32[]{:S(2)}) async-start(), calls=%async_computation.8 | async-start | bytes 4718592 | tf_op jit(solution)/shard_map/reduce_scatter | solution.py:31
  201.1 4.7 %copy-start = (bf16[256,2048]{1,0:T(8,128)(2,1)S(1)}, bf16[256,2048]{1,0:T(8,128)(2,1)}, u32[]{:S(2)}) copy-start(bf16[256,2048]{1,0:T(8,128)(2,1)} %all-gather.5.cloned.1.call-done) | copy-start | bytes 3145732
  205.8 179.0 %reduce-scatter.8.cloned.1.call-start = ((), (), s32[]{:S(2)}) async-start(), calls=%async_computation.9 | async-start | bytes 4718592 | tf_op jit(solution)/shard_map/reduce_scatter | solution.py:40
  209.1 203.2 %reduce-scatter.4.cloned.1.call-start = ((), (), s32[]{:S(2)}) async-start(), calls=%async_computation.7 | async-start | bytes 1310720 | tf_op jit(solution)/shard_map/reduce_scatter | solution.py:27
Sparse Core Ops, SparseCore 0:
  9.5 19.4 all-gather.8
  31.1 72.7 all-gather.10
  105.5 15.2 all-gather.4
  122.7 74.6 all-gather.6
  205.9 86.9 reduce-scatter.5
  296.3 88.3 reduce-scatter.7
  387.8 24.4 reduce-scatter.3
where the time goes:
time: 419 us
  waiting for transfers between devices  352 us (84%)
  blocking collectives  27.4 us (7%)
  matrix products  20 us (5%)
  between operations  14.2 us (3%)
    reduce_scatter x1, waiting for transfers between devices, on_device(): lax.psum_scatter(lax.dot_general(cols, act, (((0,), (0,)), ((), ())), pre...  81.7 us
    reduce_scatter x1, waiting for transfers between devices, on_device(): lax.psum_scatter(lax.dot_general(cols, dpre, (((0,), (0,)), ((), ())), pr...  79.1 us
    all_gather x1, waiting for transfers between devices, on_device(): lax.all_gather(down_weight, 'fs', axis=1, tiled=True)  76.6 us
    all_gather x1, waiting for transfers between devices, on_device(): up_local = lax.all_gather(up_weight, 'fs', axis=0, tiled=True)  74.9 us
    psum x1, blocking collectives, on_device(): down_norms = lax.psum(jnp.sum(down_grad * down_grad, axis=1), 'fs')  20.6 us
    all_gather x1, waiting for transfers between devices, on_device(): lax.all_gather(tokens, 'tp', axis=1, tiled=True)  19 us
    all_gather x1, waiting for transfers between devices, on_device(): lax.all_gather(grad_out, 'tp', axis=1, tiled=True)  13.1 us
  transfers between devices with their start and end apart: 7, of which 7 were waited for; matrix products, arithmetic and copies ran while one was open for 4% of the time, Pallas kernels for 0%

commit v1 on v0

--- a/solution.py
+++ b/solution.py
@@ -9,7 +9,12 @@
         lax.all_gather(tokens, "tp", axis=1, tiled=True),
         lax.all_gather(grad_out, "tp", axis=1, tiled=True),
     )
-    up_local = lax.all_gather(up_weight, "fs", axis=0, tiled=True)
+    ring = [up_weight]
+    for hop in range(7):
+        ring.append(lax.ppermute(ring[-1], "fs", [(dev, (dev + 1) % 8) for dev in range(8)]))
+    up_local = jnp.roll(
+        jnp.concatenate(ring[::-1], axis=0), (lax.axis_index("fs") + 1) * ring[0].shape[0], axis=0
+    )
     dact = lax.dot_general(
         cotan,
         lax.all_gather(down_weight, "fs", axis=1, tiled=True),

time: 419 us -> 393 us (0.938)
  waiting for transfers between devices: 352 us -> 304 us
  local copies, waits for them, and re-layouts: 2.22 us -> 19.7 us
    ppermute x0 -> x7, waiting for transfers between devices: none -> 143 us  [on_device(): lax.ppermute(ring[-1], 'fs', [(dev, (dev + 1) % 8) for dev in range(8)])]
    all_gather x1, waiting for transfers between devices: 76.6 us -> 0.02 us  [on_device(): lax.all_gather(down_weight, 'fs', axis=1, tiled=True)]
    all_gather x1 -> x0, waiting for transfers between devices: 74.9 us -> none  [on_device(): up_local = lax.all_gather(up_weight, 'fs', axis=0, tiled=True)]
    all_gather x1, waiting for transfers between devices: 19 us -> 0.01 us  [on_device(): lax.all_gather(tokens, 'tp', axis=1, tiled=True)]
    unnamed x3 -> x20, local copies, waits for them, and re-layouts: 2.22 us -> 18.8 us
    all_gather x1, waiting for transfers between devices: 13.1 us -> 0.02 us  [on_device(): lax.all_gather(grad_out, 'tp', axis=1, tiled=True)]
    reduce_scatter x1, waiting for transfers between devices: 4.82 us -> 17.3 us  [on_device(): lax.psum_scatter(rounded.astype(jnp.float32).astype(jnp.bfloat16), 'tp',...]
    reduce_scatter x1, waiting for transfers between devices: 79.1 us -> 68.6 us  [on_device(): lax.psum_scatter(lax.dot_general(cols, dpre, (((0,), (0,)), ((), ())), pr...]
  transfers between devices with their start and end apart: 7 -> 13, of which waited for: 7 -> 10; matrix products, arithmetic and copies ran while one was open for 4% -> 11% of each run, Pallas kernels for 0% -> 0%
where the time goes in v1:
time: 393 us
  waiting for transfers between devices  304 us (77%)
  blocking collectives  28 us (7%)
  matrix products  20.7 us (5%)
  local copies, waits for them, and re-layouts  19.7 us (5%)
  between operations  14.2 us (4%)
    ppermute x7, waiting for transfers between devices, on_device(): lax.ppermute(ring[-1], 'fs', [(dev, (dev + 1) % 8) for dev in range(8)])  143 us
    reduce_scatter x1, waiting for transfers between devices, on_device(): lax.psum_scatter(lax.dot_general(cols, act, (((0,), (0,)), ((), ())), pre...  72.2 us
    reduce_scatter x1, waiting for transfers between devices, on_device(): lax.psum_scatter(lax.dot_general(cols, dpre, (((0,), (0,)), ((), ())), pr...  68.6 us
    psum x1, blocking collectives, on_device(): down_norms = lax.psum(jnp.sum(down_grad * down_grad, axis=1), 'fs')  21.3 us
    unnamed x20, local copies, waits for them, and re-layouts  18.8 us
    reduce_scatter x1, waiting for transfers between devices, on_device(): lax.psum_scatter(rounded.astype(jnp.float32).astype(jnp.bfloat16), 'tp',...  17.3 us
  transfers between devices with their start and end apart: 13, of which 10 were waited for; matrix products, arithmetic and copies ran while one was open for 11% of the time, Pallas kernels for 0%

profile of v1, /device:TPU:0, one launch (start us, length us, event | category | flops | bytes accessed | tf_op | source)
XLA Modules:
  0.0 392.7 jit_solution(16833318764412643)
XLA Ops:
  9.4 3.0 collective-permute-start
  12.5 15.2 %collective-permute-done = bf16[256,1024]{1,0:T(8,128)(2,1)S(1)} collective-permute-done((bf16[256,1024]{1,0:T(8,128)(2,1)}, bf16[256,1024]{1,0:T(8,128)(2,1)S(1)}, u32[]{:S(2)}, u32[]{:S(2)}) %collective-permute-start) | collective-permute-done | bytes 524320 | tf_op jit(solution)/shard_map/ppermute | solution.py:14
  27.6 15.8 %collective-permute-done.1 = bf16[256,1024]{1,0:T(8,128)(2,1)S(1)} collective-permute-done((bf16[256,1024]{1,0:T(8,128)(2,1)S(1)}, bf16[256,1024]{1,0:T(8,128)(2,1)S(1)}, u32[]{:S(2)}, u32[]{:S(2)}) %collective-permute-start.1) | collective-permute-done | bytes 524320 | tf_op jit(solution)/shard_map/ppermute | solution.py:14
  43.4 14.9 %collective-permute-done.2 = bf16[256,1024]{1,0:T(8,128)(2,1)S(1)} collective-permute-done((bf16[256,1024]{1,0:T(8,128)(2,1)S(1)}, bf16[256,1024]{1,0:T(8,128)(2,1)S(1)}, u32[]{:S(2)}, u32[]{:S(2)}) %collective-permute-start.2) | collective-permute-done | bytes 524320 | tf_op jit(solution)/shard_map/ppermute | solution.py:14
  58.3 26.4 %collective-permute-done.3 = bf16[256,1024]{1,0:T(8,128)(2,1)S(1)} collective-permute-done((bf16[256,1024]{1,0:T(8,128)(2,1)S(1)}, bf16[256,1024]{1,0:T(8,128)(2,1)S(1)}, u32[]{:S(2)}, u32[]{:S(2)}) %collective-permute-start.3) | collective-permute-done | bytes 524320 | tf_op jit(solution)/shard_map/ppermute | solution.py:14
  84.8 15.8 %collective-permute-done.4 = bf16[256,1024]{1,0:T(8,128)(2,1)S(1)} collective-permute-done((bf16[256,1024]{1,0:T(8,128)(2,1)S(1)}, bf16[256,1024]{1,0:T(8,128)(2,1)S(1)}, u32[]{:S(2)}, u32[]{:S(2)}) %collective-permute-start.4) | collective-permute-done | bytes 524320 | tf_op jit(solution)/shard_map/ppermute | solution.py:14
  100.6 27.6 %collective-permute-done.5 = bf16[256,1024]{1,0:T(8,128)(2,1)} collective-permute-done((bf16[256,1024]{1,0:T(8,128)(2,1)S(1)}, bf16[256,1024]{1,0:T(8,128)(2,1)}, u32[]{:S(2)}, u32[]{:S(2)}) %collective-permute-start.5) | collective-permute-done | bytes 524320 | tf_op jit(solution)/shard_map/ppermute | solution.py:14
  128.2 27.5 %collective-permute-done.6 = bf16[256,1024]{1,0:T(8,128)(2,1)} collective-permute-done((bf16[256,1024]{1,0:T(8,128)(2,1)}, bf16[256,1024]{1,0:T(8,128)(2,1)}, u32[]{:S(2)}, u32[]{:S(2)}) %collective-permute-start.6) | collective-permute-done | bytes 524320 | tf_op jit(solution)/shard_map/ppermute | solution.py:14
  155.7 1.9 constant_dynamic-update-slice_fusion.15
  157.6 1.9 constant_dynamic-update-slice_fusion.14
  159.4 0.8 constant_dynamic-update-slice_fusion.13
  161.1 0.8 constant_dynamic-update-slice_fusion.11
  162.0 0.8 constant_dynamic-update-slice_fusion.10
  164.4 1.9 constant_dynamic-update-slice_fusion.7
  166.3 1.9 constant_dynamic-update-slice_fusion.6
  168.2 0.8 constant_dynamic-update-slice_fusion.5
  169.9 0.8 constant_dynamic-update-slice_fusion.3
  170.7 0.8 constant_dynamic-update-slice_fusion.2
  172.3 0.9 constant_dynamic-update-slice_fusion
  173.2 3.8 fusion.10
  177.0 4.5 %convert_bitcast_fusion = bf16[2048,1024]{0,1:T(8,128)(2,1)} fusion(bf16[256,2048]{1,0:T(8,128)(2,1)} %all-gather.4.cloned.1.call-done, f32[256,1024]{1,0:T(8,128)S(1)} %fusion.10), kind=kOutput, calls=%fused_computation | convolution fusion | flops 1076363264 | bytes 6291456 | tf_op jit(solution)/shard_map/dot_general | solution.py:46
  181.7 3.5 fusion.14
  185.2 4.5 %convert_bitcast_fusion.1 = bf16[2048,1024]{0,1:T(8,128)(2,1)} fusion(bf16[256,1024]{1,0:T(8,128)(2,1)S(1)} %fusion.14, bf16[256,2048]{1,0:T(8,128)(2,1)} %all-gather.8.cloned.1.call-done), kind=kOutput, calls=%fused_computation.1 | convolution fusion | flops 1075838976 | bytes 5767168 | tf_op jit(solution)/shard_map/dot_general | solution.py:37
  189.7 4.5 %fusion.4 = bf16[256,2048]{1,0:T(8,128)(2,1)} fusion(bf16[256,1024]{1,0:T(8,128)(2,1)S(1)} %fusion.14, bf16[4096,1024]{1,0:T(8,128)(2,1)} %constant_dynamic-update-slice_fusion, s32[]{:T(128)S(6)} %select_n.14), kind=kOutput, calls=%fused_computation.6 | convolution fusion | flops 1074266112 | bytes 5767172 | tf_op jit(solution)/shard_map/dot_general | solution.py:28
  194.2 72.2 %reduce-scatter.8.cloned.1.call-done = bf16[256,1024]{0,1:T(8,128)(2,1)} async-done(((bf16[2048,1024]{0,1:T(8,128)(2,1)}), bf16[256,1024]{0,1:T(8,128)(2,1)}) %reduce-scatter.8.cloned.1.call-update) | async-done | bytes 524304 | tf_op jit(solution)/shard_map/reduce_scatter | solution.py:45
  266.5 2.1 multiply_reduce_fusion
  268.6 21.3 %psum.15 = f32[1024]{0:T(1024)} all-reduce(f32[1024]{0:T(1024)S(1)} %get-tuple-element.10), channel_id=1, replica_groups=mesh['fs'=8,'tp'=4] {'fs'}, use_global_device_ids=true, to_apply=%region_6.7 | all-reduce | flops 1024 | bytes 8192 | tf_op jit(solution)/shard_map/psum | solution.py:55
  289.8 68.6 %reduce-scatter.6.cloned.1.call-done = bf16[256,1024]{0,1:T(8,128)(2,1)} async-done(((bf16[2048,1024]{0,1:T(8,128)(2,1)}), bf16[256,1024]{0,1:T(8,128)(2,1)}) %reduce-scatter.6.cloned.1.call-update) | async-done | bytes 524304 | tf_op jit(solution)/shard_map/reduce_scatter | solution.py:36
  358.4 2.2 copy.10
  360.7 1.2 multiply_reduce_fusion.1
  361.9 6.7 %psum.14 = f32[256]{0:T(256)} all-reduce(f32[256]{0:T(256)S(1)} %multiply_reduce_fusion.1), channel_id=1, replica_groups=mesh['fs'=8,'tp'=4] {'tp'}, use_global_device_ids=true, to_apply=%region_4.5 | all-reduce | flops 256 | bytes 2048 | tf_op jit(solution)/shard_map/psum | solution.py:54
  368.6 17.3 %reduce-scatter.4.cloned.1.call-done = bf16[256,512]{1,0:T(8,128)(2,1)} async-done(((bf16[256,2048]{1,0:T(8,128)(2,1)}), bf16[256,512]{1,0:T(8,128)(2,1)}) %reduce-scatter.4.cloned.1.call-update) | async-done | bytes 262160 | tf_op jit(solution)/shard_map/reduce_scatter | solution.py:32
  (30 shorter events, 6.5 us)
Async XLA Ops:
  7.2 156.5 %copy-start = (bf16[256,1024]{1,0:T(8,128)(2,1)S(1)}, bf16[256,1024]{1,0:T(8,128)(2,1)}, u32[]{:S(2)}) copy-start(bf16[256,1024]{1,0:T(8,128)(2,1)} %param.6) | copy-start | bytes 1572868
  7.2 166.0 %all-gather.8.cloned.1.call-start = ((), (), s32[]{:S(2)}) async-start(), calls=%async_computation.5 | async-start | bytes 1310720 | tf_op jit(solution)/shard_map/all_gather | solution.py:9
  7.9 169.1 %all-gather.4.cloned.1.call-start = ((), (), s32[]{:S(2)}) async-start(), calls=%async_computation.3 | async-start | bytes 1310720 | tf_op jit(solution)/shard_map/all_gather | solution.py:10
  8.7 173.0 %all-gather.6.cloned.1.call-start = ((), (), s32[]{:S(2)}) async-start(), calls=%async_computation.4 | async-start | bytes 4718592 | tf_op jit(solution)/shard_map/all_gather | solution.py:20
  9.4 257.1 %reduce-scatter.8.cloned.1.call-start = ((), (), s32[]{:S(2)}) async-start(), calls=%async_computation.8 | async-start | bytes 4718592 | tf_op jit(solution)/shard_map/reduce_scatter | solution.py:45
  9.4 18.2 %collective-permute-start = (bf16[256,1024]{1,0:T(8,128)(2,1)}, bf16[256,1024]{1,0:T(8,128)(2,1)S(1)}, u32[]{:S(2)}, u32[]{:S(2)}) collective-permute-start(bf16[256,1024]{1,0:T(8,128)(2,1)} %param.6), channel_id=1, source_target_pairs={{0,4},{4,8},{8,12},{12,16},{16,20},{20,24},{24,28},{28,0},{1,5},{5... | collective-permute-start | bytes 1572872 | tf_op jit(solution)/shard_map/ppermute | solution.py:14
  27.6 15.8 %collective-permute-start.1 = (bf16[256,1024]{1,0:T(8,128)(2,1)S(1)}, bf16[256,1024]{1,0:T(8,128)(2,1)S(1)}, u32[]{:S(2)}, u32[]{:S(2)}) collective-permute-start(bf16[256,1024]{1,0:T(8,128)(2,1)S(1)} %collective-permute-done), channel_id=1, source_target_pairs={{0,4},{4,8},{8,12},{12,16},{16,20},{20,24},{24,28},{28,0},{1,5},{5... | collective-permute-start | bytes 1572872 | tf_op jit(solution)/shard_map/ppermute | solution.py:14
  43.4 14.9 %collective-permute-start.2 = (bf16[256,1024]{1,0:T(8,128)(2,1)S(1)}, bf16[256,1024]{1,0:T(8,128)(2,1)S(1)}, u32[]{:S(2)}, u32[]{:S(2)}) collective-permute-start(bf16[256,1024]{1,0:T(8,128)(2,1)S(1)} %collective-permute-done.1), channel_id=1, source_target_pairs={{0,4},{4,8},{8,12},{12,16},{16,20},{20,24},{24,28},{28,0},{1,5},{5... | collective-permute-start | bytes 1572872 | tf_op jit(solution)/shard_map/ppermute | solution.py:14
  58.3 26.4 %collective-permute-start.3 = (bf16[256,1024]{1,0:T(8,128)(2,1)S(1)}, bf16[256,1024]{1,0:T(8,128)(2,1)S(1)}, u32[]{:S(2)}, u32[]{:S(2)}) collective-permute-start(bf16[256,1024]{1,0:T(8,128)(2,1)S(1)} %collective-permute-done.2), channel_id=1, source_target_pairs={{0,4},{4,8},{8,12},{12,16},{16,20},{20,24},{24,28},{28,0},{1,5},{5... | collective-permute-start | bytes 1572872 | tf_op jit(solution)/shard_map/ppermute | solution.py:14
  84.8 15.8 %collective-permute-start.4 = (bf16[256,1024]{1,0:T(8,128)(2,1)S(1)}, bf16[256,1024]{1,0:T(8,128)(2,1)S(1)}, u32[]{:S(2)}, u32[]{:S(2)}) collective-permute-start(bf16[256,1024]{1,0:T(8,128)(2,1)S(1)} %collective-permute-done.3), channel_id=1, source_target_pairs={{0,4},{4,8},{8,12},{12,16},{16,20},{20,24},{24,28},{28,0},{1,5},{5... | collective-permute-start | bytes 1572872 | tf_op jit(solution)/shard_map/ppermute | solution.py:14
  100.6 27.6 %collective-permute-start.5 = (bf16[256,1024]{1,0:T(8,128)(2,1)S(1)}, bf16[256,1024]{1,0:T(8,128)(2,1)}, u32[]{:S(2)}, u32[]{:S(2)}) collective-permute-start(bf16[256,1024]{1,0:T(8,128)(2,1)S(1)} %collective-permute-done.4), channel_id=1, source_target_pairs={{0,4},{4,8},{8,12},{12,16},{16,20},{20,24},{24,28},{28,0},{1,5},{5... | collective-permute-start | bytes 1572872 | tf_op jit(solution)/shard_map/ppermute | solution.py:14
  128.2 27.5 %collective-permute-start.6 = (bf16[256,1024]{1,0:T(8,128)(2,1)}, bf16[256,1024]{1,0:T(8,128)(2,1)}, u32[]{:S(2)}, u32[]{:S(2)}) collective-permute-start(bf16[256,1024]{1,0:T(8,128)(2,1)} %collective-permute-done.5), channel_id=1, source_target_pairs={{0,4},{4,8},{8,12},{12,16},{16,20},{20,24},{24,28},{28,0},{1,5},{5... | collective-permute-start | bytes 1572872 | tf_op jit(solution)/shard_map/ppermute | solution.py:14
  177.0 4.7 %copy-start.1 = (bf16[256,2048]{1,0:T(8,128)(2,1)S(1)}, bf16[256,2048]{1,0:T(8,128)(2,1)}, u32[]{:S(2)}) copy-start(bf16[256,2048]{1,0:T(8,128)(2,1)} %all-gather.4.cloned.1.call-done) | copy-start | bytes 3145732
  181.6 176.9 %reduce-scatter.6.cloned.1.call-start = ((), (), s32[]{:S(2)}) async-start(), calls=%async_computation.7 | async-start | bytes 4718592 | tf_op jit(solution)/shard_map/reduce_scatter | solution.py:36
  189.7 196.2 %reduce-scatter.4.cloned.1.call-start = ((), (), s32[]{:S(2)}) async-start(), calls=%async_computation.6 | async-start | bytes 1310720 | tf_op jit(solution)/shard_map/reduce_scatter | solution.py:32
Sparse Core Ops, SparseCore 0:
  9.5 19.4 all-gather.7
  30.6 16.6 all-gather.3
  49.3 101.5 all-gather.5
  181.7 84.6 reduce-scatter.7
  269.9 88.4 reduce-scatter.5
  361.4 24.4 reduce-scatter.3
